TPU v7x, 32 devices: a whole 2x2x4 slice. The times are simulated.
32 devices in a mesh: sp: 4 (over x, core), tp: 8 (over z, y).
Axes of the slice: x: 2, y: 2, z: 4, core: 2. Of those that a mesh axis runs over, the one named last changes fastest.
Arguments:
- latent: bfloat16 [512, 4096], P('sp', 'tp'), may hold values from -60 to 60
- context: bfloat16 [64, 4096], P('sp', 'tp'), may hold values from -6 to 6
- conditioning: bfloat16 [4096], P('sp'), may hold values from -6 to 6
- context_prompt_vector: bfloat16 [4096], P('sp'), may hold values from -6 to 6
- shift_matrix: bfloat16 [4096, 4096], P('tp', 'sp'), may hold values from -0.09375 to 0.09375
- scale_matrix: bfloat16 [4096, 4096], P('tp', 'sp'), may hold values from -0.09375 to 0.09375
- residual_gate_matrix: bfloat16 [4096, 4096], P('tp', 'sp'), may hold values from -0.09375 to 0.09375
- query_matrix: bfloat16 [2048, 4096], P('tp'), may hold values from -0.09375 to 0.09375
- key_matrix: bfloat16 [2048, 4096], P('tp'), may hold values from -0.09375 to 0.09375
- value_matrix: bfloat16 [4096, 4096], P('tp'), may hold values from -0.09375 to 0.09375
- gate_matrix: bfloat16 [4096, 4096], P('tp'), may hold values from -0.09375 to 0.09375
- decay_down_factor: bfloat16 [2, 4096, 16], replicated, may hold values from -0.09375 to 0.09375
- decay_up_factor: bfloat16 [2, 16, 2048], replicated, may hold values from -1.5 to 1.5
- decay_key_bias: float32 [2, 2048], replicated, may hold values from -0.5 to 7
- spike_log_decay: float32 [2, 512, 16], P(None, 'sp'), may hold values from -2.8 to 0
- output_gain: float32 [4096], P('tp'), may hold values from 0.1 to 1.9
- output_matrix: bfloat16 [4096, 4096], P('tp'), may hold values from -0.375 to 0.375
Outputs:
- mixed: bfloat16 [512, 4096], P('sp', 'tp')
All inputs are finite; a program needn't handle non-finite values.
Results may differ from a plain program's by a relative error of at most 0.013.
Values may be sent and summed in bfloat16 or wider, within the bound.
A program may use at most 64 MiB of HBM per device.

v0:
```python
import jax
import jax.numpy as jnp
from jax import lax
from jax.sharding import PartitionSpec as P

D = 4096
HEADS = 16
DK = 128
DECAY_RANK = 16
BLK = 64
VGROUP = 64
epsilon = 1e-05
gate_norm = 16.0
precise = lax.Precision.HIGHEST


def for_sending(value):

    def short(part):
        return part.astype(jnp.bfloat16) if part.dtype == jnp.float32 else part

    return jax.tree.map(short, value)


def from_partner(value, axis, distance):
    return lax.ppermute(value, axis, [(i, i ^ 1 << distance) for i in range(lax.axis_size(axis))])


def carried_in(value, axis, combine, identity, reverse):
    peers, index = (lax.axis_size(axis), lax.axis_index(axis))
    everything = jax.tree.map(
        lambda part, kind: lax.all_gather(part.astype(kind), axis),
        value,
        (jnp.bfloat16, jnp.bfloat16),
    )
    start = jax.tree.map(
        lambda part, zero: jnp.broadcast_to(jnp.asarray(zero, part.dtype), part.shape),
        value,
        identity,
    )

    def turn(k, before):
        at = peers - 1 - k if reverse else k
        reached = at > index if reverse else at < index
        new = combine(
            before, jax.tree.map(lambda part, own: part[at].astype(own.dtype), everything, value)
        )
        return jax.tree.map(lambda a, b: jnp.where(reached, a, b), new, before)

    return lax.fori_loop(0, peers, turn, start)


def linear(rows, weight):
    return lax.dot_general(
        rows, weight, (((1,), (1,)), ((), ())), preferred_element_type=jnp.float32
    )


def modulated(rows, row_sum, row_squares, shift_vec, scale_vec):
    rows_f = rows.astype(jnp.float32)
    mean_val = row_sum / D
    variance = row_squares / D - mean_val * mean_val
    return (
        (rows_f - mean_val) * lax.rsqrt(variance + epsilon) * (1.0 + scale_vec) + shift_vec
    ).astype(jnp.bfloat16)


def reverse_rows(array):
    return jnp.flip(array, axis=0)


def end_state(key_rows, value_rows, log_decay):
    cumulative = jnp.cumsum(log_decay, axis=0)
    totals = cumulative[-1]
    weighted = key_rows * jnp.exp(totals - cumulative)
    return (jnp.exp(totals), jnp.einsum("nhd,nhe->hde", weighted, value_rows, precision=precise))


def combine(earlier, later):
    return (earlier[0] * later[0], later[0][..., None] * earlier[1] + later[1])


def blockwise(queries, key_rows, value_rows, log_decay, carried, block_len):
    length, head_count, _ = queries.shape
    value_width = value_rows.shape[-1]
    blocks = length // block_len

    def shaped(array):
        return array.reshape(blocks, block_len, head_count, array.shape[-1])

    triangle = jnp.tril(jnp.ones((block_len, block_len), jnp.float32))

    def advance(state_now, inputs):
        block_q, block_k, block_v, block_a = inputs
        cumulative = jnp.cumsum(block_a, axis=0)
        block_end = cumulative[-1]
        query_dec = block_q * jnp.exp(cumulative)
        scores = (
            jnp.einsum("ihd,jhd->hij", query_dec, block_k * jnp.exp(-cumulative), precision=precise)
            * triangle
        )
        result = jnp.einsum("hij,jhe->ihe", scores, block_v, precision=precise)
        result = result + jnp.einsum("ihd,hde->ihe", query_dec, state_now, precision=precise)
        state_next = state_now * jnp.exp(block_end)[:, :, None] + jnp.einsum(
            "jhd,jhe->hde", block_k * jnp.exp(block_end - cumulative), block_v, precision=precise
        )
        return (state_next, result)

    _, outputs = lax.scan(
        advance, carried, (shaped(queries), shaped(key_rows), shaped(value_rows), shaped(log_decay))
    )
    return outputs.reshape(length, head_count, value_width)


def head_channels(pieces, per_head, tp_index):
    for bit_number in range(per_head.bit_length() - 1):
        partner = from_partner(
            (for_sending(pieces[0]), for_sending(pieces[1]), for_sending(pieces[2])),
            "tp",
            bit_number,
        )
        upper = tp_index // (1 << bit_number) % 2 == 1
        pieces = tuple(
            (
                jnp.where(
                    upper,
                    jnp.concatenate([theirs, mine], axis=1),
                    jnp.concatenate([mine, theirs], axis=1),
                )
                for mine, theirs in zip(pieces, partner)
            )
        )
    return pieces


def context_totals(fwd_growth, fwd_state, bwd_growth, bwd_state, identity):

    def absorb(carried, piece):
        return (combine(carried, piece), None)

    total_fwd, _ = lax.scan(absorb, identity, (fwd_growth, fwd_state))
    total_bwd, _ = lax.scan(absorb, identity, (bwd_growth, bwd_state), reverse=True)
    return (total_fwd, total_bwd)


def stored(array):
    return lax.optimization_barrier(array.astype(jnp.bfloat16))


def local(
    latent,
    context,
    conditioning,
    context_prompt_vector,
    shift_matrix,
    scale_matrix,
    residual_gate_matrix,
    query_matrix,
    key_matrix,
    value_matrix,
    gate_matrix,
    decay_down_factor,
    decay_up_factor,
    decay_key_bias,
    spike_log_decay,
    output_gain,
    output_matrix,
):
    tp_count = lax.axis_size("tp")
    tp_index = lax.axis_index("tp")
    per_head = max(tp_count // HEADS, 1)
    heads_per_shard = max(HEADS // tp_count, 1)
    leading_head = tp_index // per_head * heads_per_shard
    tok_rows = latent.shape[0]
    conds = jax.nn.silu(
        jnp.stack([conditioning, context_prompt_vector]).astype(jnp.float32)
    ).astype(jnp.bfloat16)
    shifts, scales, gates = lax.psum(
        (
            linear(conds, shift_matrix),
            linear(conds, scale_matrix),
            linear(conds, residual_gate_matrix),
        ),
        "sp",
    )
    down_both = jnp.concatenate([decay_down_factor[0].T, decay_down_factor[1].T], axis=0)
    lat_weights = (query_matrix, key_matrix, value_matrix, gate_matrix, down_both)
    ctx_weights = (key_matrix, value_matrix, down_both)
    lat_f = latent.astype(jnp.float32)
    ctx_f = context.astype(jnp.float32)
    lat_sum, lat_squares, ctx_sum, ctx_squares = lax.psum(
        (
            jnp.sum(lat_f, axis=1, keepdims=True),
            jnp.sum(lat_f * lat_f, axis=1, keepdims=True),
            jnp.sum(ctx_f, axis=1, keepdims=True),
            jnp.sum(ctx_f * ctx_f, axis=1, keepdims=True),
        ),
        "tp",
    )
    latent_normalized = modulated(latent, lat_sum, lat_squares, shifts[0], scales[0])
    normed_ctx = modulated(context, ctx_sum, ctx_squares, shifts[1], scales[1])
    lat_piece = lax.all_gather(latent_normalized, "tp", axis=1, tiled=True)
    ctx_piece = lax.all_gather(normed_ctx, "tp", axis=1, tiled=True)
    lat_new = tuple((linear(lat_piece, weight) for weight in lat_weights))
    ctx_new = tuple((linear(ctx_piece, weight) for weight in ctx_weights))
    query_part, key_part, value_part, gate_part, low_rank_part = lat_new
    ctx_key_part, ctx_value_part, ctx_low = ctx_new
    query_full, key_full, ctx_key_full = head_channels(
        (stored(query_part), stored(key_part), stored(ctx_key_part)), per_head, tp_index
    )

    def split_heads(rows, width):
        return rows.astype(jnp.float32).reshape(rows.shape[0], heads_per_shard, width)

    value_cols = value_part.shape[1] // heads_per_shard
    queries = split_heads(query_full, DK) * DK ** (-0.5)
    key_rows = split_heads(key_full, DK)
    ctx_keys = split_heads(ctx_key_full, DK)
    values_lat = split_heads(stored(value_part), value_cols)
    values_ctx = split_heads(stored(ctx_value_part), value_cols)
    gate_rows = stored(gate_part).astype(jnp.float32)

    def per_head_decay(low_rows, direction):
        up_part = lax.dynamic_slice_in_dim(
            decay_up_factor[direction], leading_head * DK, heads_per_shard * DK, 1
        ).astype(jnp.float32)
        bias_part = lax.dynamic_slice_in_dim(
            decay_key_bias[direction], leading_head * DK, heads_per_shard * DK, 0
        )
        pre_act = jnp.dot(low_rows, up_part, precision=precise) + bias_part
        return (jax.nn.log_sigmoid(pre_act) / gate_norm).reshape(
            low_rows.shape[0], heads_per_shard, DK
        )

    decay_spikes = lax.dynamic_slice_in_dim(spike_log_decay, leading_head, heads_per_shard, 2)
    latent_forward = per_head_decay(low_rank_part[:, :DECAY_RANK], 0) + decay_spikes[0][:, :, None]
    latent_backward = per_head_decay(low_rank_part[:, DECAY_RANK:], 1) + decay_spikes[1][:, :, None]
    ctx_fwd = per_head_decay(ctx_low[:, :DECAY_RANK], 0)
    ctx_bwd = per_head_decay(ctx_low[:, DECAY_RANK:], 1)
    cf_growth, cf_state = end_state(ctx_keys, values_ctx, ctx_fwd)
    cb_growth, cb_state = end_state(
        reverse_rows(ctx_keys), reverse_rows(values_ctx), reverse_rows(ctx_bwd)
    )
    lf_growth, lf_state = end_state(key_rows, values_lat, latent_forward)
    lb_growth, lb_state = end_state(
        reverse_rows(key_rows), reverse_rows(values_lat), reverse_rows(latent_backward)
    )
    identity = (
        jnp.ones((heads_per_shard, DK), jnp.float32),
        jnp.zeros((heads_per_shard, DK, value_cols), jnp.float32),
    )
    ctx_gathered = (
        lax.all_gather(cf_growth[None].astype(jnp.bfloat16), "sp", axis=0, tiled=True).astype(
            jnp.float32
        ),
        lax.all_gather(cf_state[None].astype(jnp.bfloat16), "sp", axis=0, tiled=True).astype(
            jnp.float32
        ),
        lax.all_gather(cb_growth[None].astype(jnp.bfloat16), "sp", axis=0, tiled=True).astype(
            jnp.float32
        ),
        lax.all_gather(cb_state[None].astype(jnp.bfloat16), "sp", axis=0, tiled=True).astype(
            jnp.float32
        ),
    )
    total_fwd, total_bwd = context_totals(
        ctx_gathered[0], ctx_gathered[1], ctx_gathered[2], ctx_gathered[3], identity
    )
    prefix = carried_in((lf_growth, lf_state), "sp", combine, identity, False)
    suffix = carried_in((lb_growth, lb_state), "sp", combine, identity, True)
    start_fwd = combine(total_fwd, prefix)[1]
    start_bwd = combine(total_bwd, suffix)[1]
    zero_state = jnp.zeros((heads_per_shard, DK, value_cols), jnp.float32)

    def direction_out(query_rows, key_list, value_list, log_decay, start_state):
        local_part = blockwise(query_rows, key_list, value_list, log_decay, zero_state, BLK)
        reach = query_rows * jnp.exp(jnp.cumsum(log_decay, axis=0))
        return local_part + jnp.einsum("nhd,hde->nhe", reach, start_state, precision=precise)

    out_fwd = direction_out(queries, key_rows, values_lat, latent_forward, start_fwd)
    out_bwd = reverse_rows(
        direction_out(
            reverse_rows(queries),
            reverse_rows(key_rows),
            reverse_rows(values_lat),
            reverse_rows(latent_backward),
            start_bwd,
        )
    )
    grouped = (out_fwd + out_bwd).reshape(tok_rows, -1, VGROUP)
    grouped = grouped * lax.rsqrt(jnp.mean(grouped * grouped, axis=-1, keepdims=True) + epsilon)
    heads_out = (grouped.reshape(tok_rows, -1) * output_gain * jax.nn.silu(gate_rows)).astype(
        jnp.bfloat16
    )
    branch = linear(lax.all_gather(heads_out, "tp", axis=1, tiled=True), output_matrix)
    return (latent.astype(jnp.float32) + gates[0] * branch).astype(jnp.bfloat16)


def solution(mesh):
    placed = (
        P("sp", "tp"),
        P("sp", "tp"),
        P("sp"),
        P("sp"),
        P("tp", "sp"),
        P("tp", "sp"),
        P("tp", "sp"),
        P("tp", None),
        P("tp", None),
        P("tp", None),
        P("tp", None),
        P(),
        P(),
        P(),
        P(None, "sp", None),
        P("tp"),
        P("tp", None),
    )
    return jax.shard_map(
        local, mesh=mesh, in_specs=placed, out_specs=P("sp", "tp"), check_vma=False
    )
```

profile of v0, /device:TPU:0, one launch (start us, length us, event | category | flops | bytes accessed | tf_op | source)
XLA Modules:
  0.0 266.8 jit_solution(12194387579442730119)
XLA Ops:
  6.5 0.9 stack.10
  8.1 1.6 fusion.121
  9.7 1.6 fusion.123
  11.3 1.6 fusion.125
  12.9 1.0 convert_reduce_fusion
  14.8 13.2 %all-reduce.1 = (f32[2,512]{1,0:T(2,128)S(1)}, f32[2,512]{1,0:T(2,128)S(1)}, f32[2,512]{1,0:T(2,128)}) all-reduce(f32[2,512]{1,0:T(2,128)S(1)} %fusion.121, f32[2,512]{1,0:T(2,128)S(1)} %fusion.123, f32[2,512]{1,0:T(2,128)S(1)} %fusion.125), channel_id=1, replica_groups=mesh['sp'=4,'tp'=8] {'sp'}, use_global_device_ids=true, to_apply=%region_6.7 | all-reduce | flops 3072 | bytes 24576 | tf_op jit(solution)/shard_map/psum | solution.py:178
  28.0 21.7 %all-reduce = (f32[128,1]{0,1:T(1,128)S(1)}, f32[128,1]{0,1:T(1,128)S(1)}, f32[16,1]{0,1:T(1,128)S(1)}, f32[16,1]{0,1:T(1,128)S(1)}) all-reduce(f32[128,1]{0,1:T(1,128)S(1)} %bitcast.291, f32[128,1]{0,1:T(1,128)S(1)} %bitcast.290, f32[16,1]{0,1:T(1,128)S(1)} %bitcast.293, f32[16,1]{0,1:T(1,128)S(1)} %bitcast.292), channel_id=1, replica_groups=mesh['sp'=4,'tp'=8] {'tp'}, use_global_device_ids=true, to_apply=%region_4.5 | all-reduce | flops 288 | bytes 2304 | tf_op jit(solution)/shard_map/psum | solution.py:191
  49.7 1.7 fusion.62
  52.3 1.0 slice_bitcast_fusion.3
  53.5 31.0 %all_gather.45 = bf16[16,4096]{1,0:T(8,128)(2,1)S(1)} all-gather(bf16[16,512]{1,0:T(8,128)(2,1)S(1)} %fusion.89), channel_id=1, replica_groups=mesh['sp'=4,'tp'=8] {'tp'}, dimensions={1}, use_global_device_ids=true | all-gather | bytes 147456 | tf_op jit(solution)/shard_map/all_gather | solution.py:203
  84.9 3.4 %convolution_convert_fusion.8 = bf16[16,512]{1,0:T(8,128)(2,1)S(1)} fusion(bf16[16,4096]{1,0:T(8,128)(2,1)S(1)} %all_gather.45, bf16[512,4096]{1,0:T(8,128)(2,1)} %param.38), kind=kOutput, calls=%fused_computation.96 | convolution fusion | flops 67117056 | bytes 4341760 | tf_op jit(solution)/shard_map/dot_general | solution.py:54
  89.8 5.1 %all_gather.46 = bf16[4,2,128]{2,1,0:T(2,128)(2,1)S(1)} all-gather(bf16[1,2,128]{2,1,0:T(2,128)(2,1)S(1)} %get-tuple-element.728), channel_id=1, replica_groups=mesh['sp'=4,'tp'=8] {'sp'}, dimensions={0}, use_global_device_ids=true | all-gather | bytes 2560 | tf_op jit(solution)/shard_map/all_gather | solution.py:253
  95.8 7.3 %all-gather.1 = bf16[8,128,256]{2,1,0:T(8,128)(2,1)S(1)} all-gather(bf16[2,128,256]{2,1,0:T(8,128)(2,1)S(1)} %convolution_convert_fusion.5), channel_id=3, replica_groups=mesh['sp'=4,'tp'=8] {'sp'}, dimensions={0}, use_global_device_ids=true | all-gather | bytes 655360 | tf_op jit(solution)/shard_map/all_gather | solution.py:256
  106.9 5.0 %all_gather.51 = bf16[4,2,128]{2,1,0:T(2,128)(2,1)S(1)} all-gather(bf16[1,2,128]{2,1,0:T(2,128)(2,1)S(1)} %get-tuple-element.734), channel_id=1, replica_groups=mesh['sp'=4,'tp'=8] {'sp'}, dimensions={0}, use_global_device_ids=true | all-gather | bytes 2560 | tf_op jit(solution)/shard_map/all_gather | solution.py:259
  112.7 1.1 convolution_convert_fusion.4
  113.8 7.5 %all-gather.3 = bf16[8,128,256]{2,1,0:T(8,128)(2,1)S(1)} all-gather(bf16[2,128,256]{2,1,0:T(8,128)(2,1)S(1)} %convolution_convert_fusion.4), channel_id=5, replica_groups=mesh['sp'=4,'tp'=8] {'sp'}, dimensions={0}, use_global_device_ids=true | all-gather | bytes 655360 | tf_op jit(solution)/shard_map/all_gather | solution.py:262
  121.3 1.1 convert.9
  122.4 4.4 %while.91 = (s32[]{:T(128)}, f32[2,128,256]{2,1,0:T(8,128)S(1)}, f32[4,2,128]{2,1,0:T(2,128)S(1)}, f32[4,2,128,256]{3,2,1,0:T(8,128)}, s32[]{:T(128)}, /*index=5*/s32[]{:T(128)}, s32[]{:T(128)}) while((s32[]{:T(128)}, f32[2,128,256]{2,1,0:T(8,128)S(1)}, f32[4,2,128]{2,1,0:T(2,128)S(1)}, f32[4,2,128,256]{3,2,1,0:T(8,128)}, ...), condition=%wide.region_28.29_spmd.clone, body=%wide.region_27.28_spmd.clone.sunk | while | flops 196612 | bytes 789619 | solution.py:142
  122.4 1.1 bitcast_add_fusion.5
  123.5 1.1 bitcast_add_fusion.5
  124.6 1.1 bitcast_add_fusion.5
  125.7 1.1 bitcast_add_fusion.5
  127.5 1.8 fusion.70
  129.3 1.7 fusion.74
  131.0 1.0 fusion.72
  133.5 2.1 convolution_convert_fusion.7
  137.0 3.7 %convolution_convert_fusion.2 = bf16[128,512]{1,0:T(8,128)(2,1)S(1)} fusion(bf16[128,4096]{1,0:T(8,128)(2,1)S(1)} %copy-done.1, bf16[512,4096]{1,0:T(8,128)(2,1)} %param.38), kind=kOutput, calls=%fused_computation.85 | convolution fusion | flops 536936448 | bytes 5373952 | tf_op jit(solution)/shard_map/dot_general | solution.py:54
  142.3 3.1 %convolution_convert_fusion.6 = bf16[128,256]{1,0:T(8,128)(2,1)} fusion(bf16[128,4096]{1,0:T(8,128)(2,1)S(1)} %copy-done.1, bf16[256,4096]{1,0:T(8,128)(2,1)} %param.36), kind=kOutput, calls=%fused_computation.94 | convolution fusion | flops 268468224 | bytes 3211264 | tf_op jit(solution)/shard_map/dot_general | solution.py:54
  145.4 1.6 reshape.143
  146.9 1.5 broadcast_multiply_fusion
  148.4 4.4 %convolution_convert_fusion = bf16[128,512]{1,0:T(8,128)(2,1)} fusion(bf16[128,4096]{1,0:T(8,128)(2,1)S(1)} %copy-done.1, bf16[512,4096]{1,0:T(8,128)(2,1)} %param.39), kind=kOutput, calls=%fused_computation.83 | convolution fusion | flops 536936448 | bytes 5373952 | tf_op jit(solution)/shard_map/dot_general | solution.py:54
  152.8 1.0 reshape.144
  153.8 1.0 broadcast_add_fusion
  154.9 1.0 rev.32
  155.9 1.0 copy.163
  157.7 1.1 fusion.83
  158.9 2.3 exponential_multiply_fusion.2
  161.9 5.9 %while.89 = (s32[]{:T(128)}, f32[2,128,256]{2,1,0:T(8,128)S(1)}, f32[2,64,2,256]{3,1,0,2:T(8,128)}, f32[2,64,2,128]{3,2,1,0:T(2,128)S(1)}, f32[2,64,2,128]{3,2,1...) while((s32[]{:T(128)}, f32[2,128,256]{2,1,0:T(8,128)S(1)}, ...), condition=%wide.region_22.23_spmd.clone, body=%wide.region_20.22_spmd.clone.sunk | while | flops 139837440 | bytes 2366588 | solution.py:109
  162.0 1.0 bitcast_multiply_fusion.9
  163.9 0.9 fusion.210
  164.9 1.0 bitcast_multiply_fusion.9
  166.9 0.9 fusion.210
  167.8 1.9 copy.96
  169.7 5.1 %all_gather.48 = bf16[4,2,128]{2,1,0:T(2,128)(2,1)S(1)} all-gather(bf16[1,2,128]{2,1,0:T(2,128)(2,1)} %get-tuple-element.724), channel_id=1, replica_groups=mesh['sp'=4,'tp'=8] {'sp'}, dimensions={0}, use_global_device_ids=true | all-gather | bytes 2560 | tf_op jit(solution)/shard_map/all_gather | solution.py:32
  174.8 1.3 convolution_convert_fusion.1
  176.1 7.9 %all-gather.2 = bf16[8,128,256]{2,1,0:T(8,128)(2,1)} all-gather(bf16[2,128,256]{2,1,0:T(8,128)(2,1)S(1)} %convolution_convert_fusion.1), channel_id=4, replica_groups=mesh['sp'=4,'tp'=8] {'sp'}, dimensions={0}, use_global_device_ids=true | all-gather | bytes 655360 | tf_op jit(solution)/shard_map/all_gather | solution.py:32
  184.0 4.4 %while.90 = (s32[]{:T(128)}, f32[2,128]{1,0:T(2,128)S(1)}, f32[2,128,256]{2,1,0:T(8,128)S(1)}, s32[]{:T(128)}, bf16[4,2,128]{2,1,0:T(2,128)(2,1)S(1)}, /*index=5...) while((s32[]{:T(128)}, f32[2,128]{1,0:T(2,128)S(1)}, ...), condition=%wide.region_25.26_spmd.clone, body=%wide.region_24.25_spmd.clone.sunk | while | flops 328968 | bytes 660669 | solution.py:50
  184.0 1.0 fusion.211
  185.1 1.0 fusion.211
  186.2 1.0 fusion.211
  187.3 1.0 fusion.211
  188.4 2.4 fusion.46
  190.8 3.1 %rev.38 = f32[128,2,256]{0,2,1:T(8,128)} reverse(f32[128,2,256]{0,2,1:T(8,128)} %fusion.46), dimensions={0} | reverse | bytes 524288 | tf_op jit(solution)/shard_map/jit(_flip)/rev | solution.py:69
  194.0 1.1 broadcast_add_fusion.1
  195.8 4.3 %while.86 = (s32[]{:T(128)}, f32[2,128,256]{2,1,0:T(8,128)S(1)}, f32[2,64,2,256]{3,1,0,2:T(8,128)}, f32[2,64,2,128]{3,2,1,0:T(2,128)S(1)}, f32[2,64,2,128]{3,2,1...) while((s32[]{:T(128)}, f32[2,128,256]{2,1,0:T(8,128)S(1)}, ...), condition=%wide.region_9.10_spmd.clone, body=%wide.region_7.9_spmd.clone.sunk | while | flops 139837440 | bytes 2594944 | solution.py:109
  197.1 0.9 fusion.196
  199.2 0.9 fusion.196
  200.1 1.8 copy.86
  201.9 5.0 %all_gather.42 = bf16[4,2,128]{2,1,0:T(2,128)(2,1)S(1)} all-gather(bf16[1,2,128]{2,1,0:T(2,128)(2,1)S(1)} %get-tuple-element.720), channel_id=1, replica_groups=mesh['sp'=4,'tp'=8] {'sp'}, dimensions={0}, use_global_device_ids=true | all-gather | bytes 2560 | tf_op jit(solution)/shard_map/all_gather | solution.py:32
  207.3 7.6 %all-gather = bf16[8,128,256]{2,1,0:T(8,128)(2,1)S(1)} all-gather(bf16[2,128,256]{2,1,0:T(8,128)(2,1)S(1)} %convolution_convert_fusion.3), channel_id=2, replica_groups=mesh['sp'=4,'tp'=8] {'sp'}, dimensions={0}, use_global_device_ids=true | all-gather | bytes 655360 | tf_op jit(solution)/shard_map/all_gather | solution.py:32
  215.7 1.7 fusion.130
  217.8 1.7 fusion.68
  219.5 35.8 %all-gather.9.cloned.1.call-done = bf16[128,4096]{1,0:T(8,128)(2,1)} async-done(((bf16[128,512]{1,0:T(8,128)(2,1)}), bf16[128,4096]{1,0:T(8,128)(2,1)}) %all-gather.9.cloned.1.call-update) | async-done | bytes 1048592 | tf_op jit(solution)/shard_map/all_gather | solution.py:295
  255.3 4.7 %fusion.50 = bf16[128,512]{1,0:T(8,128)(2,1)} fusion(bf16[128,4096]{1,0:T(8,128)(2,1)} %all-gather.9.cloned.1.call-done, bf16[512,4096]{1,0:T(8,128)(2,1)} %param.45, bf16[128,512]{1,0:T(8,128)(2,1)S(1)} %copy-done.11, f32[512]{0:T(512)S(1)} %bitcast.285), kind=kOutput, calls=%fused_computation.87 | convolution fusion | flops 537133056 | bytes 5507072 | tf_op jit(solution)/shard_map/dot_general | solution.py:54
  (178 shorter events, 24.6 us)
Async XLA Ops:
  6.5 82.4 %copy-start = (bf16[256,4096]{1,0:T(8,128)(2,1)S(1)}, bf16[256,4096]{1,0:T(8,128)(2,1)}, u32[]{:S(2)}) copy-start(bf16[256,4096]{1,0:T(8,128)(2,1)} %param.37) | copy-start | bytes 6291460
  6.5 46.8 %copy-start.17 = (bf16[16,512]{1,0:T(8,128)(2,1)S(1)}, bf16[16,512]{1,0:T(8,128)(2,1)}, u32[]{:S(2)}) copy-start(bf16[16,512]{1,0:T(8,128)(2,1)} %param.30) | copy-start | bytes 49156
  6.5 46.7 %copy-start.16 = (bf16[2,16,2048]{2,1,0:T(8,128)(2,1)S(1)}, bf16[2,16,2048]{2,1,0:T(8,128)(2,1)}, u32[]{:S(2)}) copy-start(bf16[2,16,2048]{2,1,0:T(8,128)(2,1)} %param.41) | copy-start | bytes 393220
  6.5 121.0 %all-gather.7.cloned.1.call-start = ((), (), s32[]{:S(2)}) async-start(), calls=%async_computation | async-start | bytes 1179648 | tf_op jit(solution)/shard_map/all_gather | solution.py:202
  51.4 203.9 %all-gather.9.cloned.1.call-start = ((), (), s32[]{:S(2)}) async-start(), calls=%async_computation.1 | async-start | bytes 1179648 | tf_op jit(solution)/shard_map/all_gather | solution.py:295
  53.3 49.8 %copy-start.15 = (bf16[16,4096]{1,0:T(8,128)(2,1)}, bf16[16,4096]{1,0:T(8,128)(2,1)S(1)}, u32[]{:S(2)}) copy-start(bf16[16,4096]{1,0:T(8,128)(2,1)S(1)} %get-tuple-element.713) | copy-start | bytes 393220
  53.3 49.8 %copy-start.18 = (bf16[1,16,2048]{2,1,0:T(8,128)(2,1)}, bf16[1,16,2048]{2,1,0:T(8,128)(2,1)S(1)}, u32[]{:S(2)}) copy-start(bf16[1,16,2048]{2,1,0:T(8,128)(2,1)S(1)} %get-tuple-element.721) | copy-start | bytes 196612
  53.3 49.8 %copy-start.19 = (bf16[1,16,2048]{2,1,0:T(8,128)(2,1)}, bf16[1,16,2048]{2,1,0:T(8,128)(2,1)S(1)}, u32[]{:S(2)}) copy-start(bf16[1,16,2048]{2,1,0:T(8,128)(2,1)S(1)} %get-tuple-element.722) | copy-start | bytes 196612
  84.4 5.4 %copy-start.22 = (f32[1,256]{1,0:T(1,128)}, f32[1,256]{1,0:T(1,128)S(1)}, u32[]{:S(2)}) copy-start(f32[1,256]{1,0:T(1,128)S(1)} %get-tuple-element.747) | copy-start | bytes 3076
  103.9 0.8 copy-start.3
  126.8 0.7 copy-start.5
  127.5 9.4 %copy-start.1 = (bf16[128,4096]{1,0:T(8,128)(2,1)S(1)}, bf16[128,4096]{1,0:T(8,128)(2,1)}, u32[]{:S(2)}) copy-start(bf16[128,4096]{1,0:T(8,128)(2,1)} %all-gather.7.cloned.1.call-done) | copy-start | bytes 3145732
  152.8 9.1 %copy-start.2 = (f32[2,128,256]{2,1,0:T(8,128)S(1)}, f32[2,128,256]{2,1,0:T(8,128)}, u32[]{:S(2)}) copy-start(f32[2,128,256]{2,1,0:T(8,128)} %custom-call.4) | copy-start | bytes 786436
  161.9 22.1 %copy-start.8 = (f32[2,128,256]{2,1,0:T(8,128)S(1)}, f32[2,128,256]{2,1,0:T(8,128)}, u32[]{:S(2)}) copy-start(f32[2,128,256]{2,1,0:T(8,128)} %custom-call.6) | copy-start | bytes 786436
  167.8 20.6 %copy-start.6 = (f32[2,128,256]{2,1,0:T(8,128)S(1)}, f32[2,128,256]{2,1,0:T(8,128)}, u32[]{:S(2)}) copy-start(f32[2,128,256]{2,1,0:T(8,128)} %copy-done.5) | copy-start | bytes 786436
  167.8 28.0 %copy-start.9 = (f32[2,64,2,256]{3,2,1,0:T(2,128)S(1)}, f32[2,64,2,256]{3,2,1,0:T(2,128)}, u32[]{:S(2)}) copy-start(f32[2,64,2,256]{3,2,1,0:T(2,128)} %reshape_reshape.7) | copy-start | bytes 786436
  176.1 17.8 %copy-start.14 = (f32[128,256]{1,0:T(8,128)S(1)}, f32[128,256]{1,0:T(8,128)}, u32[]{:S(2)}) copy-start(f32[128,256]{1,0:T(8,128)} %broadcast_multiply_fusion) | copy-start | bytes 393220
  176.1 19.7 %copy-start.10 = (f32[2,64,2,128]{3,2,1,0:T(2,128)S(1)}, f32[2,64,2,128]{3,2,1,0:T(2,128)}, u32[]{:S(2)}) copy-start(f32[2,64,2,128]{3,2,1,0:T(2,128)} %reshape_reshape.6) | copy-start | bytes 393220
  195.8 11.2 %copy-start.13 = (f32[128,2,128]{2,1,0:T(2,128)S(1)}, f32[128,2,128]{2,1,0:T(2,128)}, u32[]{:S(2)}) copy-start(f32[128,2,128]{2,1,0:T(2,128)} %get-tuple-element.717) | copy-start | bytes 393220
  195.8 19.2 %copy-start.7 = (f32[2,128,256]{2,1,0:T(8,128)S(1)}, f32[2,128,256]{2,1,0:T(8,128)}, u32[]{:S(2)}) copy-start(f32[2,128,256]{2,1,0:T(8,128)} %custom-call.2) | copy-start | bytes 786436
  200.1 15.6 %copy-start.4 = (f32[2,128,256]{2,1,0:T(8,128)S(1)}, f32[2,128,256]{2,1,0:T(8,128)}, u32[]{:S(2)}) copy-start(f32[2,128,256]{2,1,0:T(8,128)} %copy-done.3) | copy-start | bytes 786436
  200.1 17.7 %copy-start.20 = (f32[512]{0:T(512)S(1)}, f32[512]{0:T(512)}, u32[]{:S(2)}) copy-start(f32[512]{0:T(512)} %param.44) | copy-start | bytes 6148
  207.3 8.4 %copy-start.12 = (f32[128,2,256]{0,2,1:T(8,128)S(1)}, f32[128,2,256]{0,2,1:T(8,128)}, u32[]{:S(2)}) copy-start(f32[128,2,256]{0,2,1:T(8,128)} %rev.38) | copy-start | bytes 786436
  207.3 12.2 %copy-start.21 = (f32[2,512]{1,0:T(2,128)S(1)}, f32[2,512]{1,0:T(2,128)}, u32[]{:S(2)}) copy-start(f32[2,512]{1,0:T(2,128)} %get-tuple-element.705) | copy-start | bytes 12292
  207.3 47.9 %copy-start.11 = (bf16[128,512]{1,0:T(8,128)(2,1)S(1)}, bf16[128,512]{1,0:T(8,128)(2,1)}, u32[]{:S(2)}) copy-start(bf16[128,512]{1,0:T(8,128)(2,1)} %param.29) | copy-start | bytes 393220
Sparse Core Ops, SparseCore 0:
  51.5 35.1 all-gather.6
  219.6 35.6 all-gather.8
where the time goes:
time: 269 us; the launch traced here: 267 us
  blocking collectives  116 us (43%)
  matrix products  46.5 us (17%)
  waiting for transfers between devices  35.8 us (13%)
  other arithmetic  28.5 us (11%)
  local copies, waits for them, and re-layouts  25 us (9%)
  between operations  13.9 us (5%)
    all_gather x1, waiting for transfers between devices, local(): lax.all_gather(heads_out, 'tp', axis=1, tiled=True)  35.8 us
    all_gather x1, blocking collectives, local(): ctx_piece = lax.all_gather(normed_ctx, 'tp', axis=1, tiled=True)  31 us
    dot_general x12, matrix products, linear(): lax.dot_general(rows, weight, (((1,), (1,)), ((), ())), preferred_element...  28.7 us
    all_gather x4, blocking collectives, carried_in(): lax.all_gather(part.astype(kind), axis)  25.6 us
    psum x1, blocking collectives, local(): lax.psum((jnp.sum(lat_f, axis=1, keepdims=True), jnp.sum(lat_f * lat_f, a...  21.7 us
    psum x1, blocking collectives, local(): lax.psum((linear(conds, shift_matrix), linear(conds, scale_matrix), linea...  13.2 us
    all_gather x1, blocking collectives, local(): lax.all_gather(cb_state[None].astype(jnp.bfloat16), 'sp', axis=0, tiled=T...  7.46 us
    all_gather x1, blocking collectives, local(): lax.all_gather(cf_state[None].astype(jnp.bfloat16), 'sp', axis=0, tiled=T...  7.28 us
  transfers between devices with their start and end apart: 2, of which 1 were waited for; matrix products, arithmetic and copies ran while one was open for 7% of the time, Pallas kernels for 0%

commit v1 on v0

--- a/solution.py
+++ b/solution.py
@@ -12,6 +12,17 @@
 epsilon = 1e-05
 gate_norm = 16.0
 precise = lax.Precision.HIGHEST
+
+
+def gather_by_hops(value, axis, dim):
+    peers = lax.axis_size(axis)
+    right = [(i, (i + 1) % peers) for i in range(peers)]
+    shards = [value]
+    for reach in range(1, peers):
+        shards = [lax.ppermute(shards[0], axis, right), *shards]
+    result = jnp.concatenate(shards, axis=dim)
+    turn = (lax.axis_index(axis) + 1) * shards[-1].shape[dim]
+    return jnp.roll(result, turn, axis=dim)
 
 
 def for_sending(value):
@@ -200,7 +211,7 @@
     latent_normalized = modulated(latent, lat_sum, lat_squares, shifts[0], scales[0])
     normed_ctx = modulated(context, ctx_sum, ctx_squares, shifts[1], scales[1])
     lat_piece = lax.all_gather(latent_normalized, "tp", axis=1, tiled=True)
-    ctx_piece = lax.all_gather(normed_ctx, "tp", axis=1, tiled=True)
+    ctx_piece = gather_by_hops(normed_ctx, "tp", 1)
     lat_new = tuple((linear(lat_piece, weight) for weight in lat_weights))
     ctx_new = tuple((linear(ctx_piece, weight) for weight in ctx_weights))
     query_part, key_part, value_part, gate_part, low_rank_part = lat_new

time: 269 us -> 283 us (1.052)
  waiting for transfers between devices: 35.8 us -> 74.8 us
  blocking collectives: 116 us -> 85.5 us
  other arithmetic: 28.5 us -> 34 us
    ppermute x0 -> x7, waiting for transfers between devices: none -> 38.5 us  [gather_by_hops(): shards = [lax.ppermute(shards[0], axis, right), *shards]]
    all_gather x1 -> x0, blocking collectives: 31 us -> none  [local(): ctx_piece = lax.all_gather(normed_ctx, 'tp', axis=1, tiled=True)]
    add x8, other arithmetic: 4.77 us -> 8.55 us  [combine(): return (earlier[0] * later[0], later[0][..., None] * earlier[1] + later[1])]
  transfers between devices with their start and end apart: 2 -> 9, of which waited for: 1 -> 8; matrix products, arithmetic and copies ran while one was open for 7% -> 9% of each run, Pallas kernels for 0% -> 0%
where the time goes in v1:
time: 283 us; the launch traced here: 282 us
  blocking collectives  85.5 us (30%)
  waiting for transfers between devices  74.8 us (26%)
  matrix products  47.2 us (17%)
  other arithmetic  34 us (12%)
  local copies, waits for them, and re-layouts  25.2 us (9%)
  between operations  14 us (5%)
    ppermute x7, waiting for transfers between devices, gather_by_hops(): shards = [lax.ppermute(shards[0], axis, right), *shards]  38.5 us
    all_gather x1, waiting for transfers between devices, local(): lax.all_gather(heads_out, 'tp', axis=1, tiled=True)  36.3 us
    dot_general x12, matrix products, linear(): lax.dot_general(rows, weight, (((1,), (1,)), ((), ())), preferred_element...  28.7 us
    all_gather x4, blocking collectives, carried_in(): lax.all_gather(part.astype(kind), axis)  25.8 us
    psum x1, blocking collectives, local(): lax.psum((jnp.sum(lat_f, axis=1, keepdims=True), jnp.sum(lat_f * lat_f, a...  21.7 us
    psum x1, blocking collectives, local(): lax.psum((linear(conds, shift_matrix), linear(conds, scale_matrix), linea...  13.2 us
    add x8, other arithmetic, combine(): return (earlier[0] * later[0], later[0][..., None] * earlier[1] + later[1])  8.55 us
    all_gather x1, blocking collectives, local(): lax.all_gather(cb_state[None].astype(jnp.bfloat16), 'sp', axis=0, tiled=T...  7.46 us
  transfers between devices with their start and end apart: 9, of which 8 were waited for; matrix products, arithmetic and copies ran while one was open for 9% of the time, Pallas kernels for 0%

profile of v1, /device:TPU:0, one launch (start us, length us, event | category | flops | bytes accessed | tf_op | source)
XLA Modules:
  0.0 281.6 jit_solution(12522485515598361080)
XLA Ops:
  8.1 1.6 fusion.127
  9.7 1.6 fusion.129
  11.3 1.6 fusion.131
  12.9 1.0 convert_reduce_fusion
  14.8 13.2 %all-reduce.1 = (f32[2,512]{1,0:T(2,128)S(1)}, f32[2,512]{1,0:T(2,128)S(1)}, f32[2,512]{1,0:T(2,128)}) all-reduce(f32[2,512]{1,0:T(2,128)S(1)} %fusion.127, f32[2,512]{1,0:T(2,128)S(1)} %fusion.129, f32[2,512]{1,0:T(2,128)S(1)} %fusion.131), channel_id=1, replica_groups=mesh['sp'=4,'tp'=8] {'sp'}, use_global_device_ids=true, to_apply=%region_6.7 | all-reduce | flops 3072 | bytes 24576 | tf_op jit(solution)/shard_map/psum | solution.py:189
  28.0 21.7 %all-reduce = (f32[128,1]{0,1:T(1,128)S(1)}, f32[128,1]{0,1:T(1,128)S(1)}, f32[16,1]{0,1:T(1,128)S(1)}, f32[16,1]{0,1:T(1,128)S(1)}) all-reduce(f32[128,1]{0,1:T(1,128)S(1)} %bitcast.292, f32[128,1]{0,1:T(1,128)S(1)} %bitcast.291, f32[16,1]{0,1:T(1,128)S(1)} %bitcast.294, f32[16,1]{0,1:T(1,128)S(1)} %bitcast.293), channel_id=1, replica_groups=mesh['sp'=4,'tp'=8] {'tp'}, use_global_device_ids=true, to_apply=%region_4.5 | all-reduce | flops 288 | bytes 2304 | tf_op jit(solution)/shard_map/psum | solution.py:202
  51.1 6.4 %collective-permute-done = bf16[16,512]{1,0:T(8,128)(2,1)S(1)} collective-permute-done((bf16[16,512]{1,0:T(8,128)(2,1)S(1)}, bf16[16,512]{1,0:T(8,128)(2,1)S(1)}, u32[]{:S(2)}, u32[]{:S(2)}) %collective-permute-start) | collective-permute-done | bytes 16416 | tf_op jit(solution)/shard_map/ppermute | solution.py:22
  57.5 1.7 fusion.62
  59.3 4.7 %collective-permute-done.1 = bf16[16,512]{1,0:T(8,128)(2,1)S(1)} collective-permute-done((bf16[16,512]{1,0:T(8,128)(2,1)S(1)}, bf16[16,512]{1,0:T(8,128)(2,1)S(1)}, u32[]{:S(2)}, u32[]{:S(2)}) %collective-permute-start.1) | collective-permute-done | bytes 16416 | tf_op jit(solution)/shard_map/ppermute | solution.py:22
  64.9 5.4 %collective-permute-done.2 = bf16[16,512]{1,0:T(8,128)(2,1)S(1)} collective-permute-done((bf16[16,512]{1,0:T(8,128)(2,1)S(1)}, bf16[16,512]{1,0:T(8,128)(2,1)S(1)}, u32[]{:S(2)}, u32[]{:S(2)}) %collective-permute-start.2) | collective-permute-done | bytes 16416 | tf_op jit(solution)/shard_map/ppermute | solution.py:22
  71.0 5.8 %collective-permute-done.3 = bf16[16,512]{1,0:T(8,128)(2,1)S(1)} collective-permute-done((bf16[16,512]{1,0:T(8,128)(2,1)S(1)}, bf16[16,512]{1,0:T(8,128)(2,1)S(1)}, u32[]{:S(2)}, u32[]{:S(2)}) %collective-permute-start.3) | collective-permute-done | bytes 16416 | tf_op jit(solution)/shard_map/ppermute | solution.py:22
  76.9 6.4 %collective-permute-done.4 = bf16[16,512]{1,0:T(8,128)(2,1)S(1)} collective-permute-done((bf16[16,512]{1,0:T(8,128)(2,1)S(1)}, bf16[16,512]{1,0:T(8,128)(2,1)S(1)}, u32[]{:S(2)}, u32[]{:S(2)}) %collective-permute-start.4) | collective-permute-done | bytes 16416 | tf_op jit(solution)/shard_map/ppermute | solution.py:22
  83.9 6.0 %collective-permute-done.5 = bf16[16,512]{1,0:T(8,128)(2,1)S(1)} collective-permute-done((bf16[16,512]{1,0:T(8,128)(2,1)S(1)}, bf16[16,512]{1,0:T(8,128)(2,1)S(1)}, u32[]{:S(2)}, u32[]{:S(2)}) %collective-permute-start.5) | collective-permute-done | bytes 16416 | tf_op jit(solution)/shard_map/ppermute | solution.py:22
  92.9 3.7 %collective-permute-done.6 = bf16[16,512]{1,0:T(8,128)(2,1)S(1)} collective-permute-done((bf16[16,512]{1,0:T(8,128)(2,1)S(1)}, bf16[16,512]{1,0:T(8,128)(2,1)S(1)}, u32[]{:S(2)}, u32[]{:S(2)}) %collective-permute-start.6) | collective-permute-done | bytes 16416 | tf_op jit(solution)/shard_map/ppermute | solution.py:22
  99.3 3.4 %convolution_convert_fusion.8 = bf16[16,512]{1,0:T(8,128)(2,1)S(1)} fusion(bf16[512,4096]{1,0:T(8,128)(2,1)} %param.38, bf16[16,8192]{1,0:T(8,128)(2,1)S(1)} %constant_dynamic-update-slice_fusion, s32[]{:T(128)S(6)} %select_n.145), kind=kOutput, calls=%fused_computation.96 | convolution fusion | flops 67117056 | bytes 4341764 | tf_op jit(solution)/shard_map/dot_general | solution.py:65
  104.4 5.1 %all_gather.42 = bf16[4,2,128]{2,1,0:T(2,128)(2,1)S(1)} all-gather(bf16[1,2,128]{2,1,0:T(2,128)(2,1)S(1)} %get-tuple-element.728), channel_id=1, replica_groups=mesh['sp'=4,'tp'=8] {'sp'}, dimensions={0}, use_global_device_ids=true | all-gather | bytes 2560 | tf_op jit(solution)/shard_map/all_gather | solution.py:264
  109.8 7.3 %all-gather.1 = bf16[8,128,256]{2,1,0:T(8,128)(2,1)S(1)} all-gather(bf16[2,128,256]{2,1,0:T(8,128)(2,1)S(1)} %convolution_convert_fusion.5), channel_id=3, replica_groups=mesh['sp'=4,'tp'=8] {'sp'}, dimensions={0}, use_global_device_ids=true | all-gather | bytes 655360 | tf_op jit(solution)/shard_map/all_gather | solution.py:267
  117.1 1.0 convert.8
  118.1 4.4 %while.88 = (s32[]{:T(128)}, f32[2,128,256]{2,1,0:T(8,128)S(1)}, f32[4,2,128]{2,1,0:T(2,128)S(1)}, f32[4,2,128,256]{3,2,1,0:T(8,128)}, s32[]{:T(128)}, /*index=5*/s32[]{:T(128)}) while((s32[]{:T(128)}, f32[2,128,256]{2,1,0:T(8,128)S(1)}, f32[4,2,128]{2,1,0:T(2,128)S(1)}, f32[4,2,128,256]{3,2,1,0:T(8,128)}, s32[]{:T(128)}, ...), condition=%wide.region_19.20_spmd.clone, body=%wide.region_18.19_spmd.clone.sunk | while | flops 196611 | bytes 789599 | solution.py:152
  118.1 1.1 bitcast_add_fusion.4
  119.2 1.1 bitcast_add_fusion.4
  120.3 1.1 bitcast_add_fusion.4
  121.4 1.1 bitcast_add_fusion.4
  122.6 5.1 %all_gather.47 = bf16[4,2,128]{2,1,0:T(2,128)(2,1)S(1)} all-gather(bf16[1,2,128]{2,1,0:T(2,128)(2,1)S(1)} %get-tuple-element.734), channel_id=1, replica_groups=mesh['sp'=4,'tp'=8] {'sp'}, dimensions={0}, use_global_device_ids=true | all-gather | bytes 2560 | tf_op jit(solution)/shard_map/all_gather | solution.py:270
  128.1 7.5 %all-gather.3 = bf16[8,128,256]{2,1,0:T(8,128)(2,1)S(1)} all-gather(bf16[2,128,256]{2,1,0:T(8,128)(2,1)S(1)} %convolution_convert_fusion.4), channel_id=5, replica_groups=mesh['sp'=4,'tp'=8] {'sp'}, dimensions={0}, use_global_device_ids=true | all-gather | bytes 655360 | tf_op jit(solution)/shard_map/all_gather | solution.py:273
  135.6 1.0 convert.9
  136.6 4.4 %while.91 = (s32[]{:T(128)}, f32[2,128,256]{2,1,0:T(8,128)S(1)}, f32[4,2,128]{2,1,0:T(2,128)S(1)}, f32[4,2,128,256]{3,2,1,0:T(8,128)}, s32[]{:T(128)}, /*index=5*/s32[]{:T(128)}, s32[]{:T(128)}) while((s32[]{:T(128)}, f32[2,128,256]{2,1,0:T(8,128)S(1)}, f32[4,2,128]{2,1,0:T(2,128)S(1)}, f32[4,2,128,256]{3,2,1,0:T(8,128)}, ...), condition=%wide.region_28.29_spmd.clone, body=%wide.region_27.28_spmd.clone.sunk | while | flops 196612 | bytes 789619 | solution.py:153
  136.6 1.1 bitcast_add_fusion.5
  137.7 1.1 bitcast_add_fusion.5
  138.8 1.1 bitcast_add_fusion.5
  140.0 1.1 bitcast_add_fusion.5
  141.7 1.8 fusion.70
  143.5 1.7 fusion.74
  145.2 1.0 fusion.72
  147.7 2.1 convolution_convert_fusion.7
  151.2 3.7 %convolution_convert_fusion.2 = bf16[128,512]{1,0:T(8,128)(2,1)S(1)} fusion(bf16[128,4096]{1,0:T(8,128)(2,1)S(1)} %copy-done.1, bf16[512,4096]{1,0:T(8,128)(2,1)} %param.38), kind=kOutput, calls=%fused_computation.85 | convolution fusion | flops 536936448 | bytes 5373952 | tf_op jit(solution)/shard_map/dot_general | solution.py:65
  156.5 3.1 %convolution_convert_fusion.6 = bf16[128,256]{1,0:T(8,128)(2,1)} fusion(bf16[128,4096]{1,0:T(8,128)(2,1)S(1)} %copy-done.1, bf16[256,4096]{1,0:T(8,128)(2,1)} %param.36), kind=kOutput, calls=%fused_computation.94 | convolution fusion | flops 268468224 | bytes 3211264 | tf_op jit(solution)/shard_map/dot_general | solution.py:65
  159.6 1.6 reshape.143
  161.1 1.5 broadcast_multiply_fusion
  162.6 4.4 %convolution_convert_fusion = bf16[128,512]{1,0:T(8,128)(2,1)} fusion(bf16[128,4096]{1,0:T(8,128)(2,1)S(1)} %copy-done.1, bf16[512,4096]{1,0:T(8,128)(2,1)} %param.39), kind=kOutput, calls=%fused_computation.83 | convolution fusion | flops 536936448 | bytes 5373952 | tf_op jit(solution)/shard_map/dot_general | solution.py:65
  168.0 1.0 broadcast_add_fusion
  171.9 1.1 fusion.83
  173.0 2.3 exponential_multiply_fusion.2
  176.0 5.9 %while.89 = (s32[]{:T(128)}, f32[2,128,256]{2,1,0:T(8,128)S(1)}, f32[2,64,2,256]{3,1,0,2:T(8,128)}, f32[2,64,2,128]{3,2,1,0:T(2,128)S(1)}, f32[2,64,2,128]{3,2,1...) while((s32[]{:T(128)}, f32[2,128,256]{2,1,0:T(8,128)S(1)}, ...), condition=%wide.region_22.23_spmd.clone, body=%wide.region_20.22_spmd.clone.sunk | while | flops 139837440 | bytes 2366588 | solution.py:120
  182.0 1.8 copy.96
  183.8 5.3 %all_gather.44 = bf16[4,2,128]{2,1,0:T(2,128)(2,1)S(1)} all-gather(bf16[1,2,128]{2,1,0:T(2,128)(2,1)} %get-tuple-element.724), channel_id=1, replica_groups=mesh['sp'=4,'tp'=8] {'sp'}, dimensions={0}, use_global_device_ids=true | all-gather | bytes 2560 | tf_op jit(solution)/shard_map/all_gather | solution.py:43
  189.1 1.3 convolution_convert_fusion.1
  190.4 7.9 %all-gather.2 = bf16[8,128,256]{2,1,0:T(8,128)(2,1)} all-gather(bf16[2,128,256]{2,1,0:T(8,128)(2,1)S(1)} %convolution_convert_fusion.1), channel_id=4, replica_groups=mesh['sp'=4,'tp'=8] {'sp'}, dimensions={0}, use_global_device_ids=true | all-gather | bytes 655360 | tf_op jit(solution)/shard_map/all_gather | solution.py:43
  198.3 4.4 %while.90 = (s32[]{:T(128)}, f32[2,128]{1,0:T(2,128)S(1)}, f32[2,128,256]{2,1,0:T(8,128)S(1)}, s32[]{:T(128)}, bf16[4,2,128]{2,1,0:T(2,128)(2,1)S(1)}, /*index=5...) while((s32[]{:T(128)}, f32[2,128]{1,0:T(2,128)S(1)}, ...), condition=%wide.region_25.26_spmd.clone, body=%wide.region_24.25_spmd.clone.sunk | while | flops 328968 | bytes 660669 | solution.py:61
  198.3 1.0 fusion.214
  199.4 1.0 fusion.214
  200.5 1.0 fusion.214
  201.6 1.0 fusion.214
  202.7 2.4 fusion.46
  205.1 3.1 %rev.38 = f32[128,2,256]{0,2,1:T(8,128)} reverse(f32[128,2,256]{0,2,1:T(8,128)} %fusion.46), dimensions={0} | reverse | bytes 524288 | tf_op jit(solution)/shard_map/jit(_flip)/rev | solution.py:80
  208.2 1.1 broadcast_add_fusion.1
  210.1 4.3 %while.86 = (s32[]{:T(128)}, f32[2,128,256]{2,1,0:T(8,128)S(1)}, f32[2,64,2,256]{3,1,0,2:T(8,128)}, f32[2,64,2,128]{3,2,1,0:T(2,128)S(1)}, f32[2,64,2,128]{3,2,1...) while((s32[]{:T(128)}, f32[2,128,256]{2,1,0:T(8,128)S(1)}, ...), condition=%wide.region_9.10_spmd.clone, body=%wide.region_7.9_spmd.clone.sunk | while | flops 139837440 | bytes 2594944 | solution.py:120
  214.4 1.8 copy.86
  216.2 5.0 %all_gather.39 = bf16[4,2,128]{2,1,0:T(2,128)(2,1)S(1)} all-gather(bf16[1,2,128]{2,1,0:T(2,128)(2,1)S(1)} %get-tuple-element.720), channel_id=1, replica_groups=mesh['sp'=4,'tp'=8] {'sp'}, dimensions={0}, use_global_device_ids=true | all-gather | bytes 2560 | tf_op jit(solution)/shard_map/all_gather | solution.py:43
  221.6 7.6 %all-gather = bf16[8,128,256]{2,1,0:T(8,128)(2,1)S(1)} all-gather(bf16[2,128,256]{2,1,0:T(8,128)(2,1)S(1)} %convolution_convert_fusion.3), channel_id=2, replica_groups=mesh['sp'=4,'tp'=8] {'sp'}, dimensions={0}, use_global_device_ids=true | all-gather | bytes 655360 | tf_op jit(solution)/shard_map/all_gather | solution.py:43
  230.0 1.7 fusion.136
  232.0 1.7 fusion.68
  233.7 36.3 %all-gather.9.cloned.1.call-done = bf16[128,4096]{1,0:T(8,128)(2,1)} async-done(((bf16[128,512]{1,0:T(8,128)(2,1)}), bf16[128,4096]{1,0:T(8,128)(2,1)}) %all-gather.9.cloned.1.call-update) | async-done | bytes 1048592 | tf_op jit(solution)/shard_map/all_gather | solution.py:306
  270.0 4.7 %fusion.50 = bf16[128,512]{1,0:T(8,128)(2,1)} fusion(bf16[128,4096]{1,0:T(8,128)(2,1)} %all-gather.9.cloned.1.call-done, bf16[512,4096]{1,0:T(8,128)(2,1)} %param.45, bf16[128,512]{1,0:T(8,128)(2,1)S(1)} %copy-done.11, f32[512]{0:T(512)S(1)} %bitcast.288), kind=kOutput, calls=%fused_computation.87 | convolution fusion | flops 537133056 | bytes 5507072 | tf_op jit(solution)/shard_map/dot_general | solution.py:65
  (213 shorter events, 36.7 us)
Async XLA Ops:
  6.5 96.2 %copy-start = (bf16[256,4096]{1,0:T(8,128)(2,1)S(1)}, bf16[256,4096]{1,0:T(8,128)(2,1)}, u32[]{:S(2)}) copy-start(bf16[256,4096]{1,0:T(8,128)(2,1)} %param.37) | copy-start | bytes 6291460
  6.5 90.1 %copy-start.16 = (bf16[16,512]{1,0:T(8,128)(2,1)S(1)}, bf16[16,512]{1,0:T(8,128)(2,1)}, u32[]{:S(2)}) copy-start(bf16[16,512]{1,0:T(8,128)(2,1)} %param.30) | copy-start | bytes 49156
  6.5 63.8 %copy-start.17 = (bf16[2,16,2048]{2,1,0:T(8,128)(2,1)S(1)}, bf16[2,16,2048]{2,1,0:T(8,128)(2,1)}, u32[]{:S(2)}) copy-start(bf16[2,16,2048]{2,1,0:T(8,128)(2,1)} %param.41) | copy-start | bytes 393220
  6.5 70.3 %copy-start.18 = (f32[2,2048]{1,0:T(2,128)S(1)}, f32[2,2048]{1,0:T(2,128)}, u32[]{:S(2)}) copy-start(f32[2,2048]{1,0:T(2,128)} %param.42) | copy-start | bytes 49156
  6.5 135.2 %all-gather.7.cloned.1.call-start = ((), (), s32[]{:S(2)}) async-start(), calls=%async_computation | async-start | bytes 1179648 | tf_op jit(solution)/shard_map/all_gather | solution.py:213
  49.7 0.5 copy-start.19
  49.7 0.6 copy-start.20
  51.1 6.4 %collective-permute-start = (bf16[16,512]{1,0:T(8,128)(2,1)S(1)}, bf16[16,512]{1,0:T(8,128)(2,1)S(1)}, u32[]{:S(2)}, u32[]{:S(2)}) collective-permute-start(bf16[16,512]{1,0:T(8,128)(2,1)S(1)} %fusion.92), channel_id=1, source_target_pairs={{0,1},{1,2},{2,3},{3,4},{4,5},{5,6},{6,7},{7,0},{8,9},{9,10},{10,1... | collective-permute-start | bytes 49160 | tf_op jit(solution)/shard_map/ppermute | solution.py:22
  57.5 6.4 %collective-permute-start.1 = (bf16[16,512]{1,0:T(8,128)(2,1)S(1)}, bf16[16,512]{1,0:T(8,128)(2,1)S(1)}, u32[]{:S(2)}, u32[]{:S(2)}) collective-permute-start(bf16[16,512]{1,0:T(8,128)(2,1)S(1)} %collective-permute-done), channel_id=1, source_target_pairs={{0,1},{1,2},{2,3},{3,4},{4,5},{5,6},{6,7},{7,0},{8,9},{9,10},{10,1... | collective-permute-start | bytes 49160 | tf_op jit(solution)/shard_map/ppermute | solution.py:22
  59.2 210.8 %all-gather.9.cloned.1.call-start = ((), (), s32[]{:S(2)}) async-start(), calls=%async_computation.1 | async-start | bytes 1179648 | tf_op jit(solution)/shard_map/all_gather | solution.py:306
  63.9 6.4 %collective-permute-start.2 = (bf16[16,512]{1,0:T(8,128)(2,1)S(1)}, bf16[16,512]{1,0:T(8,128)(2,1)S(1)}, u32[]{:S(2)}, u32[]{:S(2)}) collective-permute-start(bf16[16,512]{1,0:T(8,128)(2,1)S(1)} %collective-permute-done.1), channel_id=1, source_target_pairs={{0,1},{1,2},{2,3},{3,4},{4,5},{5,6},{6,7},{7,0},{8,9},{9,10},{10,1... | collective-permute-start | bytes 49160 | tf_op jit(solution)/shard_map/ppermute | solution.py:22
  64.9 38.5 %copy-start.15 = (bf16[16,4096]{1,0:T(8,128)(2,1)}, bf16[16,4096]{1,0:T(8,128)(2,1)S(1)}, u32[]{:S(2)}) copy-start(bf16[16,4096]{1,0:T(8,128)(2,1)S(1)} %get-tuple-element.713) | copy-start | bytes 393220
  70.4 6.5 %collective-permute-start.3 = (bf16[16,512]{1,0:T(8,128)(2,1)S(1)}, bf16[16,512]{1,0:T(8,128)(2,1)S(1)}, u32[]{:S(2)}, u32[]{:S(2)}) collective-permute-start(bf16[16,512]{1,0:T(8,128)(2,1)S(1)} %collective-permute-done.2), channel_id=1, source_target_pairs={{0,1},{1,2},{2,3},{3,4},{4,5},{5,6},{6,7},{7,0},{8,9},{9,10},{10,1... | collective-permute-start | bytes 49160 | tf_op jit(solution)/shard_map/ppermute | solution.py:22
  76.8 6.4 %collective-permute-start.4 = (bf16[16,512]{1,0:T(8,128)(2,1)S(1)}, bf16[16,512]{1,0:T(8,128)(2,1)S(1)}, u32[]{:S(2)}, u32[]{:S(2)}) collective-permute-start(bf16[16,512]{1,0:T(8,128)(2,1)S(1)} %collective-permute-done.3), channel_id=1, source_target_pairs={{0,1},{1,2},{2,3},{3,4},{4,5},{5,6},{6,7},{7,0},{8,9},{9,10},{10,1... | collective-permute-start | bytes 49160 | tf_op jit(solution)/shard_map/ppermute | solution.py:22
  83.3 6.6 %collective-permute-start.5 = (bf16[16,512]{1,0:T(8,128)(2,1)S(1)}, bf16[16,512]{1,0:T(8,128)(2,1)S(1)}, u32[]{:S(2)}, u32[]{:S(2)}) collective-permute-start(bf16[16,512]{1,0:T(8,128)(2,1)S(1)} %collective-permute-done.4), channel_id=1, source_target_pairs={{0,1},{1,2},{2,3},{3,4},{4,5},{5,6},{6,7},{7,0},{8,9},{9,10},{10,1... | collective-permute-start | bytes 49160 | tf_op jit(solution)/shard_map/ppermute | solution.py:22
  89.9 6.6 %collective-permute-start.6 = (bf16[16,512]{1,0:T(8,128)(2,1)S(1)}, bf16[16,512]{1,0:T(8,128)(2,1)S(1)}, u32[]{:S(2)}, u32[]{:S(2)}) collective-permute-start(bf16[16,512]{1,0:T(8,128)(2,1)S(1)} %collective-permute-done.5), channel_id=1, source_target_pairs={{0,1},{1,2},{2,3},{3,4},{4,5},{5,6},{6,7},{7,0},{8,9},{9,10},{10,1... | collective-permute-start | bytes 49160 | tf_op jit(solution)/shard_map/ppermute | solution.py:22
  97.4 6.1 %copy-start.23 = (f32[1,256]{1,0:T(1,128)S(1)}, f32[1,256]{1,0:T(1,128)}, u32[]{:S(2)}) copy-start(f32[1,256]{1,0:T(1,128)} %get-tuple-element.748) | copy-start | bytes 3076
  122.5 18.5 %copy-start.5 = (f32[2,128,256]{2,1,0:T(8,128)}, f32[2,128,256]{2,1,0:T(8,128)S(1)}, u32[]{:S(2)}) copy-start(f32[2,128,256]{2,1,0:T(8,128)S(1)} %get-tuple-element.462) | copy-start | bytes 786436
  122.5 21.0 %copy-start.25 = (f32[1,256]{1,0:T(1,128)S(1)}, f32[1,256]{1,0:T(1,128)}, u32[]{:S(2)}) copy-start(f32[1,256]{1,0:T(1,128)} %get-tuple-element.747) | copy-start | bytes 3076
  122.5 22.7 %copy-start.24 = (f32[1,256]{1,0:T(1,128)S(1)}, f32[1,256]{1,0:T(1,128)}, u32[]{:S(2)}) copy-start(f32[1,256]{1,0:T(1,128)} %get-tuple-element.748) | copy-start | bytes 3076
  141.1 0.7 copy-start.3
  141.7 9.5 %copy-start.1 = (bf16[128,4096]{1,0:T(8,128)(2,1)S(1)}, bf16[128,4096]{1,0:T(8,128)(2,1)}, u32[]{:S(2)}) copy-start(bf16[128,4096]{1,0:T(8,128)(2,1)} %all-gather.7.cloned.1.call-done) | copy-start | bytes 3145732
  167.0 9.0 %copy-start.2 = (f32[2,128,256]{2,1,0:T(8,128)S(1)}, f32[2,128,256]{2,1,0:T(8,128)}, u32[]{:S(2)}) copy-start(f32[2,128,256]{2,1,0:T(8,128)} %custom-call.4) | copy-start | bytes 786436
  176.0 22.2 %copy-start.8 = (f32[2,128,256]{2,1,0:T(8,128)S(1)}, f32[2,128,256]{2,1,0:T(8,128)}, u32[]{:S(2)}) copy-start(f32[2,128,256]{2,1,0:T(8,128)} %custom-call.6) | copy-start | bytes 786436
  182.0 20.7 %copy-start.4 = (f32[2,128,256]{2,1,0:T(8,128)S(1)}, f32[2,128,256]{2,1,0:T(8,128)}, u32[]{:S(2)}) copy-start(f32[2,128,256]{2,1,0:T(8,128)} %copy-done.3) | copy-start | bytes 786436
  182.0 28.1 %copy-start.9 = (f32[2,64,2,256]{3,2,1,0:T(2,128)S(1)}, f32[2,64,2,256]{3,2,1,0:T(2,128)}, u32[]{:S(2)}) copy-start(f32[2,64,2,256]{3,2,1,0:T(2,128)} %reshape_reshape.7) | copy-start | bytes 786436
  190.4 17.8 %copy-start.14 = (f32[128,256]{1,0:T(8,128)S(1)}, f32[128,256]{1,0:T(8,128)}, u32[]{:S(2)}) copy-start(f32[128,256]{1,0:T(8,128)} %broadcast_multiply_fusion) | copy-start | bytes 393220
  190.4 19.7 %copy-start.10 = (f32[2,64,2,128]{3,2,1,0:T(2,128)S(1)}, f32[2,64,2,128]{3,2,1,0:T(2,128)}, u32[]{:S(2)}) copy-start(f32[2,64,2,128]{3,2,1,0:T(2,128)} %reshape_reshape.6) | copy-start | bytes 393220
  210.1 11.2 %copy-start.13 = (f32[128,2,128]{2,1,0:T(2,128)S(1)}, f32[128,2,128]{2,1,0:T(2,128)}, u32[]{:S(2)}) copy-start(f32[128,2,128]{2,1,0:T(2,128)} %get-tuple-element.717) | copy-start | bytes 393220
  210.1 19.1 %copy-start.7 = (f32[2,128,256]{2,1,0:T(8,128)S(1)}, f32[2,128,256]{2,1,0:T(8,128)}, u32[]{:S(2)}) copy-start(f32[2,128,256]{2,1,0:T(8,128)} %custom-call.2) | copy-start | bytes 786436
  214.3 15.6 %copy-start.6 = (f32[2,128,256]{2,1,0:T(8,128)S(1)}, f32[2,128,256]{2,1,0:T(8,128)}, u32[]{:S(2)}) copy-start(f32[2,128,256]{2,1,0:T(8,128)} %copy-done.5) | copy-start | bytes 786436
  214.4 17.7 %copy-start.21 = (f32[512]{0:T(512)S(1)}, f32[512]{0:T(512)}, u32[]{:S(2)}) copy-start(f32[512]{0:T(512)} %param.44) | copy-start | bytes 6148
  221.5 8.4 %copy-start.12 = (f32[128,2,256]{0,2,1:T(8,128)S(1)}, f32[128,2,256]{0,2,1:T(8,128)}, u32[]{:S(2)}) copy-start(f32[128,2,256]{0,2,1:T(8,128)} %rev.38) | copy-start | bytes 786436
  221.6 12.2 %copy-start.22 = (f32[2,512]{1,0:T(2,128)S(1)}, f32[2,512]{1,0:T(2,128)}, u32[]{:S(2)}) copy-start(f32[2,512]{1,0:T(2,128)} %get-tuple-element.705) | copy-start | bytes 12292
  221.6 48.4 %copy-start.11 = (bf16[128,512]{1,0:T(8,128)(2,1)S(1)}, bf16[128,512]{1,0:T(8,128)(2,1)}, u32[]{:S(2)}) copy-start(bf16[128,512]{1,0:T(8,128)(2,1)} %param.29) | copy-start | bytes 393220
Sparse Core Ops, SparseCore 0:
  59.3 40.6 all-gather.6
  233.8 36.1 all-gather.8
